TPU v7x, 256 devices: a whole 4x4x8 slice. The times are simulated.
256 devices in a mesh: sp: 32 (over z, y), tp: 8 (over x, core).
Axes of the slice: x: 4, y: 4, z: 8, core: 2. Of those that a mesh axis runs over, the one named last changes fastest.
Arguments:
- skip_stream: bfloat16 [24576, 2048], P(('sp', 'tp')), may hold values from -24 to 24
- acceptance_signal: bfloat16 [24576, 2048], P('sp', 'tp'), may hold values from -6 to 6
- lookup_mapped: bfloat16 [24576, 2048], P('sp', 'tp'), may hold values from -12 to 12
- payload_mapped: bfloat16 [24576, 2048], P('sp', 'tp'), may hold values from -6 to 6
- result_switch: bfloat16 [24576, 2048], P('sp', 'tp'), may hold values from -6 to 6
- forget_dynamic_share: bfloat16 [24576, 2048], P('sp', 'tp'), may hold values from -4 to 4
- additive_forget_logarithm: float32 [24576, 32], P('sp', 'tp'), may hold values from -1 to 0
- forget_feature_offset: float32 [2048], P('tp'), may hold values from -11 to -3
- substitution_dynamic_share: bfloat16 [24576, 2048], P('sp', 'tp'), may hold values from -6 to 6
- substitution_feature_offset: float32 [2048], P('tp'), may hold values from -6.5 to 2.5
- diagonal_reward_scales: float32 [2048], P('tp'), may hold values from -0.9 to 0.9
- result_matrix: bfloat16 [2048, 2048], P('tp'), may hold values from -0.125 to 0.125
- mlp_rescaler: float32 [2048], replicated, may hold values from 0.1 to 1.9
- switch_matrix: bfloat16 [2048, 5120], P('sp', 'tp'), may hold values from -0.125 to 0.125
- expand_matrix: bfloat16 [2048, 5120], P('sp', 'tp'), may hold values from -0.125 to 0.125
- contract_matrix: bfloat16 [2048, 5120], P('sp', 'tp'), may hold values from -0.25 to 0.25
Outputs:
- mixed_out: bfloat16 [24576, 2048], P(('sp', 'tp'))
All inputs are finite; a program needn't handle non-finite values.
Results may differ from a plain program's by a relative error of at most 0.015.
Values may be sent and summed in bfloat16 or wider, within the bound.
A program may use at most 128 MiB of HBM per device.

v0:
```python
import jax
import jax.numpy as jnp
from jax import lax
from jax.sharding import Mesh
from jax.sharding import PartitionSpec as P

PER_GROUP_DIMS = 64
SP = ("sp_0", "sp_1")
SP_TP = ("sp_0", "sp_1", "tp")
norm_eps = 1e-06
group_eps = 0.00064
half_step = 0.5


def side_by_side(arrays, axis, dim, along):
    widths = [a.shape[along] for a in arrays]
    both = jnp.concatenate(arrays, axis=along)
    result = lax.all_gather(both, axis, axis=dim, tiled=True)
    return tuple(jnp.split(result, [sum(widths[:k]) for k in range(1, len(widths))], axis=along))


def filled_with(shard, identity):
    return jax.tree.map(
        lambda a, e: jnp.broadcast_to(jnp.asarray(e, a.dtype), a.shape), shard, identity
    )


def carried_in(shard, axes, combine, identity):
    before = start = filled_with(shard, identity)
    so_far = shard
    for axis in reversed(axes):
        peers, place = (lax.axis_size(axis), lax.axis_index(axis))
        pieces = jax.tree.map(
            lambda part, kind: lax.all_gather(part.astype(kind), axis),
            so_far,
            (jnp.bfloat16, jnp.bfloat16),
        )
        inside, so_far = (start, start)
        for k in range(peers):
            passed = k < place
            so_far = combine(
                so_far, jax.tree.map(lambda part, own: part[k].astype(own.dtype), pieces, shard)
            )
            inside = jax.tree.map(lambda new, old: jnp.where(passed, new, old), so_far, inside)
        before = combine(inside, before)
    return before


def split_up(shard, dim, peers):
    before, after = (shard.shape[:dim], shard.shape[dim + 1 :])
    return jnp.moveaxis(shard.reshape(*before, peers, -1, *after), dim, 0)


def sent_and_summed(shard, axis, dim):
    peers = lax.axis_size(axis)
    parts = lax.all_to_all(split_up(shard, dim, peers), axis, 0, 0, tiled=True)
    return jnp.sum(parts.astype(jnp.float32), axis=0)


def compose(earlier, latter):
    prod_first, carry_first = earlier
    prod_second, carry_second = latter
    product = jnp.einsum("hij,hjk->hik", prod_first, prod_second)
    carried = jnp.einsum("hij,hjk->hik", carry_first, prod_second) + carry_second
    return (product, carried)


def masked_pairs(left, right, keep):
    return jnp.where(keep, jnp.einsum("htc,hjc->htj", left, right), 0.0)


def block_step(carry, inputs):
    state_part, transition = carry
    read_blk, logstep_blk, key_blk, value_blk, unit_blk, rate_blk = inputs
    length = read_blk.shape[1]
    width = value_blk.shape[2]
    cumulate = jnp.cumsum(logstep_blk, axis=1)
    growth = jnp.exp(cumulate)
    shrink = jnp.exp(-cumulate)
    before_unit = jnp.exp(cumulate - logstep_blk) * unit_blk
    erase_dir = unit_blk * rate_blk
    key_back = key_blk * shrink
    erase_back = erase_dir * shrink
    read_fwd = read_blk * growth
    end_growth = growth[:, -1:, :]
    key_end = key_back * end_growth
    erase_end = erase_back * end_growth
    row_index = lax.broadcasted_iota(jnp.int32, (length, length), 0)
    col_index = lax.broadcasted_iota(jnp.int32, (length, length), 1)
    strict = col_index < row_index
    inclusive = col_index <= row_index
    key_past = masked_pairs(before_unit, key_back, strict)
    erase_past = masked_pairs(before_unit, erase_back, strict)
    key_read = masked_pairs(read_fwd, key_back, inclusive)
    erase_read = masked_pairs(read_fwd, erase_back, inclusive)
    recall_rhs = jnp.einsum("htk,hvk->htv", before_unit, state_part) + jnp.einsum(
        "htj,hjv->htv", key_past, value_blk
    )
    solved = jax.scipy.linalg.solve_triangular(
        erase_past,
        jnp.concatenate([recall_rhs, before_unit], axis=-1),
        lower=True,
        unit_diagonal=True,
    )
    recalled = solved[..., :width]
    carried_map = solved[..., width:]
    local_out = (
        jnp.einsum("htk,hvk->htv", read_fwd, state_part)
        + jnp.einsum("htj,hjv->htv", key_read, value_blk)
        - jnp.einsum("htj,hjv->htv", erase_read, recalled)
    )
    from_start = read_fwd - jnp.einsum("htj,hjk->htk", erase_read, carried_map)
    coefficient = jnp.einsum("htk,hjk->htj", from_start, transition)
    new_state = (
        state_part * end_growth
        + jnp.einsum("htv,htk->hvk", value_blk, key_end)
        - jnp.einsum("htv,htk->hvk", recalled, erase_end)
    )
    step_map = jnp.eye(width, dtype=jnp.float32)[None] * end_growth - jnp.einsum(
        "htj,htk->hjk", carried_map, erase_end
    )
    new_transition = jnp.einsum("hij,hjk->hik", transition, step_map)
    return ((new_state, new_transition), (local_out, coefficient))


def per_device(
    skip_stream,
    acceptance_signal,
    lookup_mapped,
    payload_mapped,
    result_switch,
    forget_dynamic_share,
    additive_forget_logarithm,
    forget_feature_offset,
    substitution_dynamic_share,
    substitution_feature_offset,
    diagonal_reward_scales,
    result_matrix,
    mlp_rescaler,
    switch_matrix,
    expand_matrix,
    contract_matrix,
):
    matrix_length, matrix_breadth = acceptance_signal.shape
    attention_groups = matrix_breadth // PER_GROUP_DIMS
    gate_whole, up_whole, down_whole = side_by_side(
        (switch_matrix, expand_matrix, contract_matrix), SP, 0, 1
    )

    def by_head(values):
        return values.astype(jnp.float32).reshape(matrix_length, attention_groups, PER_GROUP_DIMS)

    acceptance_lines = by_head(acceptance_signal)
    lookup_vectors = by_head(lookup_mapped)
    payload_vectors = by_head(payload_mapped)
    log_decay_rate = (
        -jax.nn.softplus(
            -(forget_feature_offset[None, :] + forget_dynamic_share.astype(jnp.float32))
        )
        - 0.5
    )
    log_step = (
        -jnp.exp(log_decay_rate).reshape(matrix_length, attention_groups, PER_GROUP_DIMS)
        + additive_forget_logarithm[:, :, None]
    )
    replace_rate = jax.nn.sigmoid(
        substitution_feature_offset[None, :] + substitution_dynamic_share.astype(jnp.float32)
    )
    replace_rate = replace_rate.reshape(matrix_length, attention_groups, PER_GROUP_DIMS)
    unit_key = lookup_vectors * lax.rsqrt(
        jnp.sum(lookup_vectors * lookup_vectors, axis=-1, keepdims=True) + norm_eps
    )
    block_len = min(64, matrix_length)
    block_count = matrix_length // block_len

    def to_blocks(values):
        return values.reshape(block_count, block_len, attention_groups, PER_GROUP_DIMS).transpose(
            0, 2, 1, 3
        )

    def from_blocks(values):
        return values.transpose(0, 2, 1, 3).reshape(matrix_length, attention_groups, PER_GROUP_DIMS)

    identity_mats = jnp.broadcast_to(
        jnp.eye(PER_GROUP_DIMS, dtype=jnp.float32),
        (attention_groups, PER_GROUP_DIMS, PER_GROUP_DIMS),
    )
    zero_mats = jnp.zeros((attention_groups, PER_GROUP_DIMS, PER_GROUP_DIMS), jnp.float32)
    (closing_state, closing_map), (local_blocks, coef_blocks) = lax.scan(
        block_step,
        (zero_mats, identity_mats),
        (
            to_blocks(acceptance_lines),
            to_blocks(log_step),
            to_blocks(lookup_vectors),
            to_blocks(payload_vectors),
            to_blocks(unit_key),
            to_blocks(replace_rate),
        ),
    )
    _, carried = carried_in((closing_map, closing_state), SP, compose, (identity_mats, zero_mats))
    outcome = from_blocks(local_blocks) + jnp.einsum(
        "hvk,thk->thv", carried, from_blocks(coef_blocks)
    )
    centre = jnp.mean(outcome, axis=-1, keepdims=True)
    spread = jnp.mean(jnp.square(outcome - centre), axis=-1, keepdims=True)
    rescaled_attention = (outcome - centre) * lax.rsqrt(spread + group_eps)
    diagonal_reward_summand = (
        jnp.sum(
            acceptance_lines
            * lookup_vectors
            * diagonal_reward_scales.reshape(attention_groups, PER_GROUP_DIMS),
            axis=-1,
            keepdims=True,
        )
        * payload_vectors
    )
    merged_attention = (
        (rescaled_attention + diagonal_reward_summand).reshape(matrix_length, matrix_breadth)
        * result_switch.astype(jnp.float32)
    ).astype(jnp.bfloat16)
    row_block = merged_attention
    projected = sent_and_summed(
        jnp.dot(row_block, result_matrix, preferred_element_type=jnp.float32).astype(jnp.bfloat16),
        "tp",
        0,
    ).astype(jnp.bfloat16)
    stream = skip_stream.astype(jnp.float32) + lax.optimization_barrier(projected).astype(
        jnp.float32
    )
    scale_rows = lax.rsqrt(jnp.mean(stream * stream, axis=-1, keepdims=True) + norm_eps)
    normed_rows = (stream * scale_rows * mlp_rescaler[None, :]).astype(jnp.bfloat16)
    whole_rows = lax.all_gather(normed_rows, "tp", axis=0, tiled=True)
    gate_act = jnp.dot(whole_rows, gate_whole, preferred_element_type=jnp.float32)
    up_act = jnp.dot(whole_rows, up_whole, preferred_element_type=jnp.float32)
    hidden = (jax.nn.silu(gate_act) * up_act).astype(jnp.bfloat16)
    row_block = hidden
    ffn_out = lax.psum_scatter(
        lax.dot_general(
            row_block, down_whole, (((1,), (1,)), ((), ())), preferred_element_type=jnp.float32
        ).astype(jnp.bfloat16),
        "tp",
        scatter_dimension=0,
        tiled=True,
    )
    return (stream + half_step * lax.optimization_barrier(ffn_out).astype(jnp.float32)).astype(
        jnp.bfloat16
    )


def solution(mesh):
    torus = Mesh(mesh.devices.reshape(8, 4, mesh.shape["tp"]), ("sp_0", "sp_1", "tp"))
    in_specs = (
        P(SP_TP, None),
        P(SP, "tp"),
        P(SP, "tp"),
        P(SP, "tp"),
        P(SP, "tp"),
        P(SP, "tp"),
        P(SP, "tp"),
        P("tp"),
        P(SP, "tp"),
        P("tp"),
        P("tp"),
        P("tp", None),
        P(),
        P(SP, "tp"),
        P(SP, "tp"),
        P(SP, "tp"),
    )
    out_specs = P(SP_TP, None)
    return jax.shard_map(
        per_device, mesh=torus, in_specs=in_specs, out_specs=out_specs, check_vma=False
    )
```

profile of v0, /device:TPU:8, one launch (start us, length us, event | category | flops | bytes accessed | tf_op | source)
XLA Modules:
  0.0 707.8 jit_solution(7916593708579089121)
XLA Ops:
  10.1 2.5 reshape_reshape.12
  12.6 2.1 copy.77
  19.0 1.9 neg.31
  28.2 4.9 multiply_bitcast_fusion
  33.1 339.6 %while.17 = (s32[]{:T(128)}, f32[4,64,64]{2,1,0:T(8,128)S(1)}, bf16[4,64,64]{1,2,0:T(8,128)(2,1)S(1)}, f32[12,4,64,64]{3,2,1,0:T(8,128)}, bf16[12,4,64,64]{3,2,1...) while((s32[]{:T(128)}, f32[4,64,64]{2,1,0:T(8,128)S(1)}, ...), condition=%wide.region_3.4_spmd.clone, body=%wide.region_1.3_spmd.clone.sunk | while | flops 58290240 | bytes 4974245 | solution.py:189
  38.1 19.7 %custom-call.9 = f32[4,1,64,64]{2,3,1,0:T(8,128)S(1)} custom-call(f32[4,1,64,64]{3,2,1,0:T(8,128)S(1)} %fusion.259), custom_call_target="InvertDiagBlocksLowerTriangular" | custom-call | tf_op jit(solution)/shard_map/while/body/eval_jaxpr/jit(_solve_triangular)/vmap()/triangular_solve | solution.py:99
  66.4 19.7 %custom-call.9 = f32[4,1,64,64]{2,3,1,0:T(8,128)S(1)} custom-call(f32[4,1,64,64]{3,2,1,0:T(8,128)S(1)} %fusion.259), custom_call_target="InvertDiagBlocksLowerTriangular" | custom-call | tf_op jit(solution)/shard_map/while/body/eval_jaxpr/jit(_solve_triangular)/vmap()/triangular_solve | solution.py:99
  94.7 19.7 %custom-call.9 = f32[4,1,64,64]{2,3,1,0:T(8,128)S(1)} custom-call(f32[4,1,64,64]{3,2,1,0:T(8,128)S(1)} %fusion.259), custom_call_target="InvertDiagBlocksLowerTriangular" | custom-call | tf_op jit(solution)/shard_map/while/body/eval_jaxpr/jit(_solve_triangular)/vmap()/triangular_solve | solution.py:99
  123.0 19.7 %custom-call.9 = f32[4,1,64,64]{2,3,1,0:T(8,128)S(1)} custom-call(f32[4,1,64,64]{3,2,1,0:T(8,128)S(1)} %fusion.259), custom_call_target="InvertDiagBlocksLowerTriangular" | custom-call | tf_op jit(solution)/shard_map/while/body/eval_jaxpr/jit(_solve_triangular)/vmap()/triangular_solve | solution.py:99
  151.3 19.7 %custom-call.9 = f32[4,1,64,64]{2,3,1,0:T(8,128)S(1)} custom-call(f32[4,1,64,64]{3,2,1,0:T(8,128)S(1)} %fusion.259), custom_call_target="InvertDiagBlocksLowerTriangular" | custom-call | tf_op jit(solution)/shard_map/while/body/eval_jaxpr/jit(_solve_triangular)/vmap()/triangular_solve | solution.py:99
  179.6 19.7 %custom-call.9 = f32[4,1,64,64]{2,3,1,0:T(8,128)S(1)} custom-call(f32[4,1,64,64]{3,2,1,0:T(8,128)S(1)} %fusion.259), custom_call_target="InvertDiagBlocksLowerTriangular" | custom-call | tf_op jit(solution)/shard_map/while/body/eval_jaxpr/jit(_solve_triangular)/vmap()/triangular_solve | solution.py:99
  207.9 19.7 %custom-call.9 = f32[4,1,64,64]{2,3,1,0:T(8,128)S(1)} custom-call(f32[4,1,64,64]{3,2,1,0:T(8,128)S(1)} %fusion.259), custom_call_target="InvertDiagBlocksLowerTriangular" | custom-call | tf_op jit(solution)/shard_map/while/body/eval_jaxpr/jit(_solve_triangular)/vmap()/triangular_solve | solution.py:99
  236.2 19.7 %custom-call.9 = f32[4,1,64,64]{2,3,1,0:T(8,128)S(1)} custom-call(f32[4,1,64,64]{3,2,1,0:T(8,128)S(1)} %fusion.259), custom_call_target="InvertDiagBlocksLowerTriangular" | custom-call | tf_op jit(solution)/shard_map/while/body/eval_jaxpr/jit(_solve_triangular)/vmap()/triangular_solve | solution.py:99
  264.5 19.7 %custom-call.9 = f32[4,1,64,64]{2,3,1,0:T(8,128)S(1)} custom-call(f32[4,1,64,64]{3,2,1,0:T(8,128)S(1)} %fusion.259), custom_call_target="InvertDiagBlocksLowerTriangular" | custom-call | tf_op jit(solution)/shard_map/while/body/eval_jaxpr/jit(_solve_triangular)/vmap()/triangular_solve | solution.py:99
  292.8 19.7 %custom-call.9 = f32[4,1,64,64]{2,3,1,0:T(8,128)S(1)} custom-call(f32[4,1,64,64]{3,2,1,0:T(8,128)S(1)} %fusion.259), custom_call_target="InvertDiagBlocksLowerTriangular" | custom-call | tf_op jit(solution)/shard_map/while/body/eval_jaxpr/jit(_solve_triangular)/vmap()/triangular_solve | solution.py:99
  321.1 19.7 %custom-call.9 = f32[4,1,64,64]{2,3,1,0:T(8,128)S(1)} custom-call(f32[4,1,64,64]{3,2,1,0:T(8,128)S(1)} %fusion.259), custom_call_target="InvertDiagBlocksLowerTriangular" | custom-call | tf_op jit(solution)/shard_map/while/body/eval_jaxpr/jit(_solve_triangular)/vmap()/triangular_solve | solution.py:99
  349.4 19.7 %custom-call.9 = f32[4,1,64,64]{2,3,1,0:T(8,128)S(1)} custom-call(f32[4,1,64,64]{3,2,1,0:T(8,128)S(1)} %fusion.259), custom_call_target="InvertDiagBlocksLowerTriangular" | custom-call | tf_op jit(solution)/shard_map/while/body/eval_jaxpr/jit(_solve_triangular)/vmap()/triangular_solve | solution.py:99
  372.8 12.5 %all-gather = bf16[16,64,64]{2,1,0:T(8,128)(2,1)S(1)} all-gather(bf16[4,64,64]{2,1,0:T(8,128)(2,1)S(1)} %copy.76), channel_id=2, replica_groups=mesh['sp_0'=8,'sp_1'=4,'tp'=8] {'sp_1'}, dimensions={0}, use_global_device_ids=true | all-gather | bytes 163840 | tf_op jit(solution)/shard_map/all_gather | solution.py:34
  385.3 12.3 %all-gather.2 = bf16[16,64,64]{2,1,0:T(8,128)(2,1)S(1)} all-gather(bf16[4,64,64]{2,1,0:T(8,128)(2,1)S(1)} %convert_element_type.170), channel_id=4, replica_groups=mesh['sp_0'=8,'sp_1'=4,'tp'=8] {'sp_1'}, dimensions={0}, use_global_device_ids=true | all-gather | bytes 163840 | tf_op jit(solution)/shard_map/all_gather | solution.py:34
  400.0 29.3 %all-gather.3 = bf16[32,64,64]{2,1,0:T(8,128)(2,1)S(1)} all-gather(bf16[4,64,64]{2,1,0:T(8,128)(2,1)S(1)} %convolution_add_fusion.10), channel_id=5, replica_groups=mesh['sp_0'=8,'sp_1'=4,'tp'=8] {'sp_0'}, dimensions={0}, use_global_device_ids=true | all-gather | bytes 294912 | tf_op jit(solution)/shard_map/all_gather | solution.py:34
  430.4 25.5 %all-gather.1 = bf16[32,64,64]{2,1,0:T(8,128)(2,1)S(1)} all-gather(bf16[4,64,64]{2,1,0:T(8,128)(2,1)S(1)} %fusion.143), channel_id=3, replica_groups=mesh['sp_0'=8,'sp_1'=4,'tp'=8] {'sp_0'}, dimensions={0}, use_global_device_ids=true | all-gather | bytes 294912 | tf_op jit(solution)/shard_map/all_gather | solution.py:34
  459.5 2.2 copy.74
  463.1 1.9 copy.75
  466.6 2.0 fusion.73
  474.0 42.6 %all_to_all.5 = bf16[8,96,2048]{2,1,0:T(8,128)(2,1)} all-to-all(bf16[8,96,2048]{2,1,0:T(8,128)(2,1)S(1)} %bitcast.166), channel_id=1, replica_groups=mesh['sp_0'=8,'sp_1'=4,'tp'=8] {'tp'}, dimensions={0} | all-to-all | bytes 6291456 | tf_op jit(solution)/shard_map/all_to_all | solution.py:56
  516.7 2.5 reduce_sum.61
  521.5 26.1 %all-gather.7.cloned.1.call-done = bf16[768,2048]{1,0:T(8,128)(2,1)} async-done(((bf16[96,2048]{1,0:T(8,128)(2,1)}), bf16[768,2048]{1,0:T(8,128)(2,1)}) %all-gather.7.cloned.1.call-update) | async-done | bytes 3145744 | tf_op jit(solution)/shard_map/all_gather | solution.py:233
  547.6 96.5 %all-gather.9.cloned.1.call-done = bf16[2048,1920]{1,0:T(8,128)(2,1)} async-done(((bf16[64,1920]{1,0:T(8,128)(2,1)}), bf16[2048,1920]{1,0:T(8,128)(2,1)}) %all-gather.9.cloned.1.call-update) | async-done | bytes 7864336 | tf_op jit(solution)/shard_map/all_gather | solution.py:18
  644.2 6.6 fusion.62
  650.8 11.6 %convolution_convert_fusion = bf16[768,2048]{1,0:T(8,128)(2,1)} fusion(bf16[2048,1920]{1,0:T(8,128)(2,1)} %all-gather.9.cloned.1.call-done, f32[768,640]{1,0:T(8,128)} %fusion.62, bf16[768,2048]{1,0:T(8,128)(2,1)} %all-gather.7.cloned.1.call-done), kind=kOutput, calls=%fused_computation.82 | convolution fusion | flops 4031053824 | bytes 13500416 | tf_op jit(solution)/shard_map/dot_general | solution.py:239
  662.4 37.0 %reduce-scatter.2.cloned.1.call-done = bf16[96,2048]{1,0:T(8,128)(2,1)} async-done(((bf16[768,2048]{1,0:T(8,128)(2,1)}), bf16[96,2048]{1,0:T(8,128)(2,1)}) %reduce-scatter.2.cloned.1.call-update) | async-done | bytes 393232 | tf_op jit(solution)/shard_map/reduce_scatter | solution.py:238
  699.4 1.9 add_convert_fusion
  (444 shorter events, 134.6 us)
Async XLA Ops:
  6.5 466.5 %copy-start = (bf16[256,2048]{1,0:T(8,128)(2,1)S(1)}, bf16[256,2048]{1,0:T(8,128)(2,1)}, u32[]{:S(2)}) copy-start(bf16[256,2048]{1,0:T(8,128)(2,1)} %param.29) | copy-start | bytes 3145732
  6.5 2.2 copy-start.7
  6.5 541.1 %all-gather.7.cloned.1.call-start = ((), (), s32[]{:S(2)}) async-start(), calls=%async_computation.2 | async-start | bytes 3538944 | tf_op jit(solution)/shard_map/all_gather | solution.py:233
  12.6 3.9 copy-start.27
  12.6 4.9 copy-start.8
  12.6 4.9 copy-start.30
  28.1 4.9 copy-start.23
  397.7 31.9 %copy-start.10 = (bf16[4,64,64]{2,1,0:T(8,128)(2,1)}, bf16[4,64,64]{2,1,0:T(8,128)(2,1)S(1)}, u32[]{:S(2)}) copy-start(bf16[4,64,64]{2,1,0:T(8,128)(2,1)S(1)} %fusion.116) | copy-start | bytes 98308
  397.9 0.6 copy-start.25
  399.2 0.6 copy-start.18
  429.3 28.8 %copy-start.4 = (bf16[32,64,64]{2,1,0:T(8,128)(2,1)}, bf16[32,64,64]{2,1,0:T(8,128)(2,1)S(1)}, u32[]{:S(2)}) copy-start(bf16[32,64,64]{2,1,0:T(8,128)(2,1)S(1)} %all-gather.3) | copy-start | bytes 786436
  429.8 0.6 copy-start.9
  455.9 2.2 copy-start.5
  456.0 0.7 copy-start.24
  456.8 4.8 copy-start.11
  457.0 4.7 copy-start.12
  457.2 4.5 copy-start.13
  457.3 0.6 copy-start.14
  463.1 3.3 copy-start.17
  463.1 3.3 copy-start.19
  463.1 3.3 copy-start.26
  466.6 3.8 copy-start.2
  466.6 3.8 copy-start.3
  468.6 1.7 copy-start.29
  471.6 1.5 copy-start.6
  516.7 2.5 copy-start.1
  516.7 2.8 copy-start.28
  519.2 1.3 copy-start.20
  519.2 1.3 copy-start.21
  519.2 1.3 copy-start.22
  520.4 123.8 %all-gather.9.cloned.1.call-start = ((), (), s32[]{:S(2)}) async-start(), calls=%async_computation.3 | async-start | bytes 8110080 | tf_op jit(solution)/shard_map/all_gather | solution.py:18
  521.2 178.2 %reduce-scatter.2.cloned.1.call-start = ((), (), s32[]{:S(2)}) async-start(), calls=%async_computation.4 | async-start | bytes 3538944 | tf_op jit(solution)/shard_map/reduce_scatter | solution.py:238
  (2 other events, 1.2 us)
Sparse Core Ops, SparseCore 0:
  520.5 27.0 all-gather.6
  550.2 93.9 all-gather.8
  662.5 36.8 reduce-scatter.1
where the time goes:
time: 710 us; the launch traced here: 708 us
  other arithmetic  257 us (36%)
  waiting for transfers between devices  160 us (23%)
  blocking collectives  122 us (17%)
  matrix products  76.9 us (11%)
  local copies, waits for them, and re-layouts  76.8 us (11%)
  between operations  13.5 us (2%)
    another operation x36, other arithmetic, block_step(): jax.scipy.linalg.solve_triangular(erase_past, jnp.concatenate([recall_rhs...  236 us
    all_gather x1, waiting for transfers between devices, side_by_side(): result = lax.all_gather(both, axis, axis=dim, tiled=True)  96.5 us
    all_gather x4, blocking collectives, carried_in(): lax.all_gather(part.astype(kind), axis)  79.6 us
    dynamic_slice x72, local copies, waits for them, and re-layouts, per_device(): lax.scan(block_step, (zero_mats, identity_mats), (to_blocks(acceptance_li...  46.8 us
    all_to_all x1, blocking collectives, sent_and_summed(): parts = lax.all_to_all(split_up(shard, dim, peers), axis, 0, 0, tiled=True)  42.6 us
    reduce_scatter x1, waiting for transfers between devices, per_device(): lax.psum_scatter(lax.dot_general(row_block, down_whole, (((1,), (1,)), ((...  37 us
    all_gather x1, waiting for transfers between devices, per_device(): whole_rows = lax.all_gather(normed_rows, 'tp', axis=0, tiled=True)  26.1 us
  transfers between devices with their start and end apart: 3, of which 3 were waited for; matrix products, arithmetic and copies ran while one was open for 0% of the time, Pallas kernels for 0%

commit v1 on v0

--- a/solution.py
+++ b/solution.py
@@ -230,7 +230,15 @@
     )
     scale_rows = lax.rsqrt(jnp.mean(stream * stream, axis=-1, keepdims=True) + norm_eps)
     normed_rows = (stream * scale_rows * mlp_rescaler[None, :]).astype(jnp.bfloat16)
-    whole_rows = lax.all_gather(normed_rows, "tp", axis=0, tiled=True)
+    whole_rows = jnp.concatenate(
+        jax.lax.all_to_all(
+            jnp.stack([normed_rows] * jax.lax.axis_size("tp"), axis=0),
+            split_axis=0,
+            axis_name="tp",
+            concat_axis=0,
+        ),
+        0,
+    )
     gate_act = jnp.dot(whole_rows, gate_whole, preferred_element_type=jnp.float32)
     up_act = jnp.dot(whole_rows, up_whole, preferred_element_type=jnp.float32)
     hidden = (jax.nn.silu(gate_act) * up_act).astype(jnp.bfloat16)

time: 710 us -> 628 us (0.88)
  waiting for transfers between devices: 160 us -> 35.8 us
  blocking collectives: 122 us -> 164 us
    all_gather x1, waiting for transfers between devices: 96.5 us -> 0.01 us  [side_by_side(): result = lax.all_gather(both, axis, axis=dim, tiled=True)]
    all_to_all x0 -> x1, blocking collectives: none -> 41.7 us  [per_device(): jax.lax.all_to_all(jnp.stack([normed_rows] * jax.lax.axis_size('tp'), axi...]
    all_gather x1 -> x0, waiting for transfers between devices: 26.1 us -> none  [per_device(): whole_rows = lax.all_gather(normed_rows, 'tp', axis=0, tiled=True)]
  transfers between devices with their start and end apart: 3 -> 2, of which waited for: 3 -> 1; matrix products, arithmetic and copies ran while one was open for 0% -> 62% of each run, Pallas kernels for 0% -> 0%
where the time goes in v1:
time: 628 us; the launch traced here: 626 us
  other arithmetic  256 us (41%)
  blocking collectives  164 us (26%)
  local copies, waits for them, and re-layouts  77.2 us (12%)
  matrix products  77.1 us (12%)
  waiting for transfers between devices  35.8 us (6%)
  between operations  13.9 us (2%)
    another operation x36, other arithmetic, block_step(): jax.scipy.linalg.solve_triangular(erase_past, jnp.concatenate([recall_rhs...  236 us
    all_gather x4, blocking collectives, carried_in(): lax.all_gather(part.astype(kind), axis)  79.5 us
    dynamic_slice x72, local copies, waits for them, and re-layouts, per_device(): lax.scan(block_step, (zero_mats, identity_mats), (to_blocks(acceptance_li...  46.8 us
    all_to_all x1, blocking collectives, sent_and_summed(): parts = lax.all_to_all(split_up(shard, dim, peers), axis, 0, 0, tiled=True)  42.6 us
    all_to_all x1, blocking collectives, per_device(): jax.lax.all_to_all(jnp.stack([normed_rows] * jax.lax.axis_size('tp'), axi...  41.7 us
    reduce_scatter x1, waiting for transfers between devices, per_device(): lax.psum_scatter(lax.dot_general(row_block, down_whole, (((1,), (1,)), ((...  35.8 us
  transfers between devices with their start and end apart: 2, of which 1 were waited for; matrix products, arithmetic and copies ran while one was open for 62% of the time, Pallas kernels for 0%

profile of v1, /device:TPU:8, one launch (start us, length us, event | category | flops | bytes accessed | tf_op | source)
XLA Modules:
  0.0 625.9 jit_solution(9580218652307525913)
XLA Ops:
  20.1 2.9 reshape_reshape.15
  23.0 2.1 add_divide_fusion
  25.1 2.9 reshape_reshape.14
  28.0 2.6 reshape_reshape.12
  30.6 4.9 multiply_bitcast_fusion
  35.5 339.6 %while.17 = (s32[]{:T(128)}, f32[4,64,64]{2,1,0:T(8,128)S(1)}, bf16[4,64,64]{1,2,0:T(8,128)(2,1)S(1)}, f32[12,4,64,64]{3,2,1,0:T(8,128)}, bf16[12,4,64,64]{3,2,1...) while((s32[]{:T(128)}, f32[4,64,64]{2,1,0:T(8,128)S(1)}, ...), condition=%wide.region_3.4_spmd.clone, body=%wide.region_1.3_spmd.clone.sunk | while | flops 58290240 | bytes 4974245 | solution.py:189
  40.6 19.7 %custom-call.9 = f32[4,1,64,64]{2,3,1,0:T(8,128)S(1)} custom-call(f32[4,1,64,64]{3,2,1,0:T(8,128)S(1)} %fusion.259), custom_call_target="InvertDiagBlocksLowerTriangular" | custom-call | tf_op jit(solution)/shard_map/while/body/eval_jaxpr/jit(_solve_triangular)/vmap()/triangular_solve | solution.py:99
  68.9 19.7 %custom-call.9 = f32[4,1,64,64]{2,3,1,0:T(8,128)S(1)} custom-call(f32[4,1,64,64]{3,2,1,0:T(8,128)S(1)} %fusion.259), custom_call_target="InvertDiagBlocksLowerTriangular" | custom-call | tf_op jit(solution)/shard_map/while/body/eval_jaxpr/jit(_solve_triangular)/vmap()/triangular_solve | solution.py:99
  97.2 19.7 %custom-call.9 = f32[4,1,64,64]{2,3,1,0:T(8,128)S(1)} custom-call(f32[4,1,64,64]{3,2,1,0:T(8,128)S(1)} %fusion.259), custom_call_target="InvertDiagBlocksLowerTriangular" | custom-call | tf_op jit(solution)/shard_map/while/body/eval_jaxpr/jit(_solve_triangular)/vmap()/triangular_solve | solution.py:99
  125.5 19.7 %custom-call.9 = f32[4,1,64,64]{2,3,1,0:T(8,128)S(1)} custom-call(f32[4,1,64,64]{3,2,1,0:T(8,128)S(1)} %fusion.259), custom_call_target="InvertDiagBlocksLowerTriangular" | custom-call | tf_op jit(solution)/shard_map/while/body/eval_jaxpr/jit(_solve_triangular)/vmap()/triangular_solve | solution.py:99
  153.8 19.7 %custom-call.9 = f32[4,1,64,64]{2,3,1,0:T(8,128)S(1)} custom-call(f32[4,1,64,64]{3,2,1,0:T(8,128)S(1)} %fusion.259), custom_call_target="InvertDiagBlocksLowerTriangular" | custom-call | tf_op jit(solution)/shard_map/while/body/eval_jaxpr/jit(_solve_triangular)/vmap()/triangular_solve | solution.py:99
  182.0 19.7 %custom-call.9 = f32[4,1,64,64]{2,3,1,0:T(8,128)S(1)} custom-call(f32[4,1,64,64]{3,2,1,0:T(8,128)S(1)} %fusion.259), custom_call_target="InvertDiagBlocksLowerTriangular" | custom-call | tf_op jit(solution)/shard_map/while/body/eval_jaxpr/jit(_solve_triangular)/vmap()/triangular_solve | solution.py:99
  210.4 19.7 %custom-call.9 = f32[4,1,64,64]{2,3,1,0:T(8,128)S(1)} custom-call(f32[4,1,64,64]{3,2,1,0:T(8,128)S(1)} %fusion.259), custom_call_target="InvertDiagBlocksLowerTriangular" | custom-call | tf_op jit(solution)/shard_map/while/body/eval_jaxpr/jit(_solve_triangular)/vmap()/triangular_solve | solution.py:99
  238.6 19.7 %custom-call.9 = f32[4,1,64,64]{2,3,1,0:T(8,128)S(1)} custom-call(f32[4,1,64,64]{3,2,1,0:T(8,128)S(1)} %fusion.259), custom_call_target="InvertDiagBlocksLowerTriangular" | custom-call | tf_op jit(solution)/shard_map/while/body/eval_jaxpr/jit(_solve_triangular)/vmap()/triangular_solve | solution.py:99
  266.9 19.7 %custom-call.9 = f32[4,1,64,64]{2,3,1,0:T(8,128)S(1)} custom-call(f32[4,1,64,64]{3,2,1,0:T(8,128)S(1)} %fusion.259), custom_call_target="InvertDiagBlocksLowerTriangular" | custom-call | tf_op jit(solution)/shard_map/while/body/eval_jaxpr/jit(_solve_triangular)/vmap()/triangular_solve | solution.py:99
  295.2 19.7 %custom-call.9 = f32[4,1,64,64]{2,3,1,0:T(8,128)S(1)} custom-call(f32[4,1,64,64]{3,2,1,0:T(8,128)S(1)} %fusion.259), custom_call_target="InvertDiagBlocksLowerTriangular" | custom-call | tf_op jit(solution)/shard_map/while/body/eval_jaxpr/jit(_solve_triangular)/vmap()/triangular_solve | solution.py:99
  323.5 19.7 %custom-call.9 = f32[4,1,64,64]{2,3,1,0:T(8,128)S(1)} custom-call(f32[4,1,64,64]{3,2,1,0:T(8,128)S(1)} %fusion.259), custom_call_target="InvertDiagBlocksLowerTriangular" | custom-call | tf_op jit(solution)/shard_map/while/body/eval_jaxpr/jit(_solve_triangular)/vmap()/triangular_solve | solution.py:99
  351.8 19.7 %custom-call.9 = f32[4,1,64,64]{2,3,1,0:T(8,128)S(1)} custom-call(f32[4,1,64,64]{3,2,1,0:T(8,128)S(1)} %fusion.259), custom_call_target="InvertDiagBlocksLowerTriangular" | custom-call | tf_op jit(solution)/shard_map/while/body/eval_jaxpr/jit(_solve_triangular)/vmap()/triangular_solve | solution.py:99
  377.6 2.2 copy.74
  381.2 1.9 copy.75
  384.4 12.5 %all-gather = bf16[16,64,64]{2,1,0:T(8,128)(2,1)S(1)} all-gather(bf16[4,64,64]{2,1,0:T(8,128)(2,1)S(1)} %copy-done.15), channel_id=2, replica_groups=mesh['sp_0'=8,'sp_1'=4,'tp'=8] {'sp_1'}, dimensions={0}, use_global_device_ids=true | all-gather | bytes 163840 | tf_op jit(solution)/shard_map/all_gather | solution.py:34
  397.0 12.2 %all-gather.2 = bf16[16,64,64]{2,1,0:T(8,128)(2,1)S(1)} all-gather(bf16[4,64,64]{2,1,0:T(8,128)(2,1)S(1)} %copy-done.13), channel_id=4, replica_groups=mesh['sp_0'=8,'sp_1'=4,'tp'=8] {'sp_1'}, dimensions={0}, use_global_device_ids=true | all-gather | bytes 163840 | tf_op jit(solution)/shard_map/all_gather | solution.py:34
  409.8 29.2 %all-gather.3 = bf16[32,64,64]{2,1,0:T(8,128)(2,1)S(1)} all-gather(bf16[4,64,64]{2,1,0:T(8,128)(2,1)S(1)} %convolution_add_fusion.10), channel_id=5, replica_groups=mesh['sp_0'=8,'sp_1'=4,'tp'=8] {'sp_0'}, dimensions={0}, use_global_device_ids=true | all-gather | bytes 294912 | tf_op jit(solution)/shard_map/all_gather | solution.py:34
  441.3 25.5 %all-gather.1 = bf16[32,64,64]{2,1,0:T(8,128)(2,1)S(1)} all-gather(bf16[4,64,64]{2,1,0:T(8,128)(2,1)S(1)} %fusion.143), channel_id=3, replica_groups=mesh['sp_0'=8,'sp_1'=4,'tp'=8] {'sp_0'}, dimensions={0}, use_global_device_ids=true | all-gather | bytes 294912 | tf_op jit(solution)/shard_map/all_gather | solution.py:34
  470.1 2.0 fusion.73
  475.6 42.6 %all_to_all.10 = bf16[8,96,2048]{2,1,0:T(8,128)(2,1)} all-to-all(bf16[8,96,2048]{2,1,0:T(8,128)(2,1)S(1)} %bitcast.167), channel_id=1, replica_groups=mesh['sp_0'=8,'sp_1'=4,'tp'=8] {'tp'}, dimensions={0} | all-to-all | bytes 6291456 | tf_op jit(solution)/shard_map/all_to_all | solution.py:56
  518.2 2.5 reduce_sum.61
  521.5 41.7 %all_to_all.11 = bf16[8,96,2048]{2,1,0:T(8,128)(2,1)} all-to-all(bf16[8,96,2048]{2,1,0:T(8,128)(2,1)S(1)} %stack.2), channel_id=1, replica_groups=mesh['sp_0'=8,'sp_1'=4,'tp'=8] {'tp'}, dimensions={0} | all-to-all | bytes 6291456 | tf_op jit(solution)/shard_map/all_to_all | solution.py:234
  563.3 6.6 %fusion.62 = f32[768,640]{1,0:T(8,128)} fusion(bf16[768,2048]{1,0:T(8,128)(2,1)} %bitcast.171, bf16[2048,1920]{1,0:T(8,128)(2,1)} %all-gather.6.cloned.1.call-done), kind=kOutput, calls=%fused_computation.87 | convolution fusion | flops 2013265920 | bytes 7733248 | tf_op jit(solution)/shard_map/dot_general | solution.py:242
  569.8 11.6 %convolution_convert_fusion = bf16[768,2048]{1,0:T(8,128)(2,1)} fusion(bf16[2048,1920]{1,0:T(8,128)(2,1)} %all-gather.6.cloned.1.call-done, f32[768,640]{1,0:T(8,128)} %fusion.62, bf16[768,2048]{1,0:T(8,128)(2,1)} %bitcast.172), kind=kOutput, calls=%fused_computation.82 | convolution fusion | flops 4031053824 | bytes 13500416 | tf_op jit(solution)/shard_map/dot_general | solution.py:247
  581.4 35.8 %reduce-scatter.2.cloned.1.call-done = bf16[96,2048]{1,0:T(8,128)(2,1)} async-done(((bf16[768,2048]{1,0:T(8,128)(2,1)}), bf16[96,2048]{1,0:T(8,128)(2,1)}) %reduce-scatter.2.cloned.1.call-update) | async-done | bytes 393232 | tf_op jit(solution)/shard_map/reduce_scatter | solution.py:246
  617.2 1.9 add_convert_fusion
  (437 shorter events, 130.8 us)
Async XLA Ops:
  6.5 467.8 %copy-start = (bf16[256,2048]{1,0:T(8,128)(2,1)S(1)}, bf16[256,2048]{1,0:T(8,128)(2,1)}, u32[]{:S(2)}) copy-start(bf16[256,2048]{1,0:T(8,128)(2,1)} %param.29) | copy-start | bytes 3145732
  6.5 556.7 %all-gather.6.cloned.1.call-start = ((), (), s32[]{:S(2)}) async-start(), calls=%async_computation.3 | async-start | bytes 8110080 | tf_op jit(solution)/shard_map/all_gather | solution.py:18
  8.3 608.8 %reduce-scatter.2.cloned.1.call-start = ((), (), s32[]{:S(2)}) async-start(), calls=%async_computation.4 | async-start | bytes 3538944 | tf_op jit(solution)/shard_map/reduce_scatter | solution.py:246
  9.6 3.2 copy-start.9
  9.6 3.2 copy-start.27
  11.8 4.4 copy-start.23
  19.0 6.0 copy-start.1
  30.6 4.9 copy-start.21
  35.5 339.6 %copy-start.7 = (bf16[768,256]{1,0:T(8,128)(2,1)S(1)}, bf16[768,256]{1,0:T(8,128)(2,1)}, u32[]{:S(2)}) copy-start(bf16[768,256]{1,0:T(8,128)(2,1)} %param.21) | copy-start | bytes 1179652
  381.2 2.6 copy-start.26
  381.2 3.2 copy-start.15
  381.2 15.7 %copy-start.13 = (bf16[4,64,64]{2,1,0:T(8,128)(2,1)S(1)}, bf16[4,64,64]{2,1,0:T(8,128)(2,1)}, u32[]{:S(2)}) copy-start(bf16[4,64,64]{2,1,0:T(8,128)(2,1)} %convert_element_type.170) | copy-start | bytes 98308
  439.1 0.6 copy-start.14
  439.9 0.6 copy-start.10
  440.5 0.6 copy-start.11
  441.3 27.9 %copy-start.12 = (bf16[4,64,64]{2,1,0:T(8,128)(2,1)}, bf16[4,64,64]{2,1,0:T(8,128)(2,1)S(1)}, u32[]{:S(2)}) copy-start(bf16[4,64,64]{2,1,0:T(8,128)(2,1)S(1)} %fusion.143) | copy-start | bytes 98308
  441.3 30.8 %copy-start.5 = (f32[768,4,64]{0,2,1:T(8,128)S(1)}, f32[768,4,64]{0,2,1:T(8,128)}, u32[]{:S(2)}) copy-start(f32[768,4,64]{0,2,1:T(8,128)} %reshape.108) | copy-start | bytes 2359300
  466.8 2.4 copy-start.6
  467.0 0.7 copy-start.22
  467.8 1.4 copy-start.16
  468.0 1.3 copy-start.17
  468.1 1.1 copy-start.18
  468.3 1.0 copy-start.19
  468.4 0.8 copy-start.20
  470.1 3.4 copy-start.2
  472.1 1.4 copy-start.4
  472.1 1.4 copy-start.25
  473.6 1.0 copy-start.8
  518.2 2.5 copy-start.3
  518.2 2.8 copy-start.24
Sparse Core Ops, SparseCore 0:
  9.9 97.6 all-gather.5
  581.5 35.5 reduce-scatter.1
